TPU v7x, 32 devices: a whole 2x2x4 slice. The times are simulated.
32 devices in a mesh: sp: 16 (over z, y, core), tp: 2 (over x).
Axes of the slice: x: 2, y: 2, z: 4, core: 2. Of those that a mesh axis runs over, the one named last changes fastest.
Arguments:
- queries: bfloat16 [3072, 1024], P('sp', 'tp'), may hold values from -6 to 6
- keys: bfloat16 [3072, 512], P('sp', 'tp'), may hold values from -6 to 6
- values: bfloat16 [3072, 512], P('sp', 'tp'), may hold values from -6 to 6
- q_gain: float32 [64], replicated, may hold values from 0.1 to 6.5
- k_gain: float32 [64], replicated, may hold values from 0.1 to 6.5
- w_out: bfloat16 [1024, 2048], P('tp'), may hold values from -12 to 12
- residual: bfloat16 [3072, 2048], P(('sp', 'tp')), may hold values from -6 to 6
- norm_gain: float32 [2048], replicated, may hold values from 0.1 to 1.9
- w_gate: bfloat16 [2048, 5632], P('sp', 'tp'), may hold values from -0.125 to 0.125
- w_up: bfloat16 [2048, 5632], P('sp', 'tp'), may hold values from -0.125 to 0.125
- w_down: bfloat16 [5632, 2048], P('tp', 'sp'), may hold values from -0.25 to 0.25
Outputs:
- layer_out: bfloat16 [3072, 2048], P(('sp', 'tp'))
All inputs are finite; a program needn't handle non-finite values.
Results may differ from a plain program's by a relative error of at most 0.018.
The roundings to bfloat16 on the way count: a program that leaves them out, or rounds other values in their place, can miss the bound.
Values may be sent and summed in bfloat16 or wider, within the bound.
A program may use at most 128 MiB of HBM per device.

v0:
```python
import math
import jax
import jax.numpy as jnp
from jax import lax
from jax.sharding import PartitionSpec as P

GRID_W = 128
EPS = 1e-06
THETA = 10000.0


def turn_half(part, angle):
    quarter = part.shape[-1] // 2
    cos_table = jnp.cos(angle)[:, None, :]
    sin_table = jnp.sin(angle)[:, None, :]
    first_part = part[..., :quarter]
    second_part = part[..., quarter:]
    return jnp.concatenate(
        [
            first_part * cos_table - second_part * sin_table,
            first_part * sin_table + second_part * cos_table,
        ],
        axis=-1,
    )


def head_norm_rope(flat, gain, offset, head_count):
    tok_rows = flat.shape[0]
    head_size = flat.shape[1] // head_count
    heads = flat.astype(jnp.float32).reshape(tok_rows, head_count, head_size)
    heads = heads * lax.rsqrt(jnp.mean(heads * heads, axis=-1, keepdims=True) + EPS) * gain
    positions = offset + jnp.arange(tok_rows, dtype=jnp.int32)
    row_pos = (positions // GRID_W).astype(jnp.float32)
    col_pos = (positions % GRID_W).astype(jnp.float32)
    half_size = head_size // 2
    inv_freq = THETA ** (-jnp.arange(0, half_size, 2, dtype=jnp.float32) / half_size)
    turned = jnp.concatenate(
        [
            turn_half(heads[..., :half_size], row_pos[:, None] * inv_freq[None, :]),
            turn_half(heads[..., half_size:], col_pos[:, None] * inv_freq[None, :]),
        ],
        axis=-1,
    )
    return turned.reshape(tok_rows, head_count * head_size).astype(jnp.bfloat16)


def body(queries, keys, values, q_gain, k_gain, w_out, residual, norm_gain, w_gate, w_up, w_down):
    tok_rows = queries.shape[0]
    head_size = q_gain.shape[0]
    q_heads = queries.shape[1] // head_size
    kv_heads = keys.shape[1] // head_size
    q_group = q_heads // kv_heads
    offset = lax.axis_index("sp") * tok_rows
    q_rot = head_norm_rope(queries, q_gain, offset, q_heads)
    k_rot = head_norm_rope(keys, k_gain, offset, kv_heads)
    query_groups = q_rot.reshape(tok_rows, kv_heads, q_group, head_size)
    score_scale = head_size ** (-0.5)
    start_state = (
        jnp.full((kv_heads, q_group, tok_rows), -1e30, jnp.float32),
        jnp.zeros((kv_heads, q_group, tok_rows), jnp.float32),
        jnp.zeros((kv_heads, q_group, tok_rows, head_size), jnp.float32),
    )
    running = start_state
    key_piece = lax.all_gather(k_rot, "sp", axis=0, tiled=True)
    value_piece = lax.all_gather(values, "sp", axis=0, tiled=True)
    piece_len = key_piece.shape[0]
    block_len = math.gcd(piece_len, 512)
    blocks = piece_len // block_len
    key_blocks = key_piece.reshape(blocks, block_len, kv_heads, head_size)
    value_blocks = value_piece.reshape(blocks, block_len, kv_heads, head_size)

    def update(state, block_pair):
        prior_max, totals, accum = state
        key_block, value_block = block_pair
        scores = (
            jnp.einsum(
                "qhgd,khd->hgqk", query_groups, key_block, preferred_element_type=jnp.float32
            )
            * score_scale
        )
        new_max = jnp.maximum(prior_max, jnp.max(scores, axis=-1))
        weights = jnp.exp(scores - new_max[..., None])
        factor = jnp.exp(prior_max - new_max)
        totals = totals * factor + jnp.sum(weights, axis=-1)
        accum = accum * factor[..., None] + jnp.einsum(
            "hgqk,khd->hgqd",
            weights.astype(jnp.bfloat16),
            value_block,
            preferred_element_type=jnp.float32,
        )
        return ((new_max, totals, accum), None)

    running, unused = lax.scan(update, running, (key_blocks, value_blocks))
    final_max, totals, accum = running
    mixed = accum / totals[..., None]
    attn = (
        jnp.transpose(mixed, (2, 0, 1, 3))
        .reshape(tok_rows, q_heads * head_size)
        .astype(jnp.bfloat16)
    )
    own_rows = lax.all_to_all(attn, "tp", split_axis=0, concat_axis=1, tiled=True)
    columns = own_rows
    proj = jnp.dot(
        columns, lax.all_gather(w_out, "tp", axis=0, tiled=True), preferred_element_type=jnp.float32
    )
    mid = residual.astype(jnp.float32) + proj
    normed = (
        mid * lax.rsqrt(jnp.mean(mid * mid, axis=-1, keepdims=True) + EPS) * norm_gain
    ).astype(jnp.bfloat16)
    gathered = lax.all_gather(normed, "tp", axis=0, tiled=True)
    columns = gathered
    gate = jnp.dot(
        columns,
        lax.all_gather(w_gate, "sp", axis=0, tiled=True),
        preferred_element_type=jnp.float32,
    )
    up_part = jnp.dot(
        columns, lax.all_gather(w_up, "sp", axis=0, tiled=True), preferred_element_type=jnp.float32
    )
    hidden = (jax.nn.silu(gate) * up_part).astype(jnp.bfloat16)
    terms = jnp.dot(
        hidden, lax.all_gather(w_down, "sp", axis=1, tiled=True), preferred_element_type=jnp.float32
    )
    down = lax.psum_scatter(
        terms.astype(jnp.bfloat16), "tp", scatter_dimension=0, tiled=True
    ).astype(jnp.float32)
    return (mid + 0.5 * down).astype(jnp.bfloat16)


def solution(mesh):
    return jax.shard_map(
        body,
        mesh=mesh,
        in_specs=(
            P("sp", "tp"),
            P("sp", "tp"),
            P("sp", "tp"),
            P(),
            P(),
            P("tp", None),
            P(("sp", "tp"), None),
            P(),
            P("sp", "tp"),
            P("sp", "tp"),
            P("tp", "sp"),
        ),
        out_specs=P(("sp", "tp"), None),
        check_vma=False,
    )
```

profile of v0, /device:TPU:0, one launch (start us, length us, event | category | flops | bytes accessed | tf_op | source)
XLA Modules:
  0.0 477.9 jit_solution(934830852998414411)
XLA Ops:
  6.6 1.0 copy.23
  7.7 0.7 fusion.24
  8.4 0.2 multiply_cosine_fusion.1
  8.7 0.7 copy.24
  9.5 0.7 all-gather.9.cloned.1.call-update
  10.3 0.7 all-gather.11.cloned.1.call-update
  11.0 0.5 all-gather.13.cloned.1.call-update
  11.6 0.5 all-gather.15.cloned.1.call-update
  12.2 0.5 all-gather.17.cloned.1.call-update
  12.8 0.1 copy.26
  12.9 0.1 fusion.21
  13.1 0.1 fusion.22
  13.2 0.1 subtract_convert_fusion.1
  13.3 38.7 %all-gather.7.cloned.1.call-done = bf16[3072,256]{1,0:T(8,128)(2,1)} async-done(((bf16[192,256]{1,0:T(8,128)(2,1)}), bf16[3072,256]{1,0:T(8,128)(2,1)}) %all-gather.7.cloned.1.call-update) | async-done | bytes 1572880 | tf_op jit(solution)/shard_map/all_gather | solution.py:64
  52.0 4.6 reshape.207
  56.6 3.3 copy.28
  59.9 32.7 %all-gather.9.cloned.1.call-done = bf16[3072,256]{1,0:T(8,128)(2,1)} async-done(((bf16[192,256]{1,0:T(8,128)(2,1)}), bf16[3072,256]{1,0:T(8,128)(2,1)}) %all-gather.9.cloned.1.call-update) | async-done | bytes 1572880 | tf_op jit(solution)/shard_map/all_gather | solution.py:65
  92.6 4.6 reshape.208
  97.2 3.3 copy.29
  100.5 32.2 %while.15 = (s32[]{:T(128)}, f32[4,2,192]{2,1,0:T(2,128)S(1)}, f32[4,2,192]{2,1,0:T(2,128)S(1)}, f32[4,2,192,64]{2,3,1,0:T(8,128)}, bf16[6,512,4,64]{1,3,2,0:T(8...) while((s32[]{:T(128)}, f32[4,2,192]{2,1,0:T(2,128)S(1)}, ...), condition=%wide.region_5.6_spmd.clone, body=%wide.region_2.5_spmd.clone.sunk | while | flops 207920640 | bytes 14189729 | solution.py:93
  100.5 1.7 bitcast_reduce_fusion.2
  102.3 0.9 fusion.50
  103.2 0.1 copy-done
  103.4 1.8 fusion.52
  105.2 0.8 copy-done.1
  106.0 1.7 bitcast_reduce_fusion.2
  107.7 0.9 fusion.50
  108.7 0.1 copy-done
  108.7 1.8 fusion.52
  110.5 0.8 copy-done.1
  111.4 1.7 bitcast_reduce_fusion.2
  113.1 0.9 fusion.50
  114.1 1.8 fusion.52
  115.9 0.8 copy-done.1
  116.7 1.7 bitcast_reduce_fusion.2
  118.4 0.9 fusion.50
  119.4 0.1 copy-done
  119.4 1.8 fusion.52
  121.3 0.8 copy-done.1
  122.1 1.7 bitcast_reduce_fusion.2
  123.8 0.9 fusion.50
  124.7 0.1 copy-done
  124.8 1.8 fusion.52
  126.6 0.8 copy-done.1
  127.4 1.7 bitcast_reduce_fusion.2
  129.1 0.9 fusion.50
  130.1 0.1 copy-done
  130.2 1.8 fusion.52
  132.0 0.8 copy-done.1
  132.8 1.1 fusion.25
  133.9 0.2 convert_element_type.65
  134.0 0.2 copy.30
  134.2 10.3 %all_to_all.16 = bf16[2,96,512]{2,1,0:T(8,128)(2,1)S(1)} all-to-all(bf16[2,96,512]{2,1,0:T(8,128)(2,1)S(1)} %copy.30), channel_id=1, replica_groups=mesh['sp'=16,'tp'=2] {'tp'}, dimensions={0} | all-to-all | bytes 393216 | tf_op jit(solution)/shard_map/all_to_all | solution.py:101
  144.5 7.2 %all-gather.11.cloned.1.call-done = bf16[1024,2048]{1,0:T(8,128)(2,1)} async-done(((bf16[512,2048]{1,0:T(8,128)(2,1)}), bf16[1024,2048]{1,0:T(8,128)(2,1)}) %all-gather.11.cloned.1.call-update) | async-done | bytes 4194320 | tf_op jit(solution)/shard_map/all_gather | solution.py:104
  151.7 3.2 multiply_reduce_fusion
  154.9 0.1 multiply_convert_fusion
  155.1 11.5 %all_gather.24 = bf16[192,2048]{1,0:T(8,128)(2,1)S(1)} all-gather(bf16[96,2048]{1,0:T(8,128)(2,1)S(1)} %multiply_convert_fusion), channel_id=1, replica_groups=mesh['sp'=16,'tp'=2] {'tp'}, dimensions={0}, use_global_device_ids=true | all-gather | bytes 1179648 | tf_op jit(solution)/shard_map/all_gather | solution.py:110
  166.6 81.3 %all-gather.13.cloned.1.call-done = bf16[2048,2816]{1,0:T(8,128)(2,1)} async-done(((bf16[128,2816]{1,0:T(8,128)(2,1)}), bf16[2048,2816]{1,0:T(8,128)(2,1)}) %all-gather.13.cloned.1.call-update) | async-done | bytes 11534352 | tf_op jit(solution)/shard_map/all_gather | solution.py:114
  247.9 8.0 %fusion.30 = f32[192,2816]{1,0:T(8,128)} fusion(bf16[192,2048]{1,0:T(8,128)(2,1)S(1)} %all_gather.24, bf16[2048,2816]{1,0:T(8,128)(2,1)} %all-gather.13.cloned.1.call-done), kind=kOutput, calls=%fused_computation.69 | convolution fusion | flops 2214592512 | bytes 14483456 | tf_op jit(solution)/shard_map/dot_general | solution.py:112
  255.9 86.4 %all-gather.15.cloned.1.call-done = bf16[2048,2816]{1,0:T(8,128)(2,1)} async-done(((bf16[128,2816]{1,0:T(8,128)(2,1)}), bf16[2048,2816]{1,0:T(8,128)(2,1)}) %all-gather.15.cloned.1.call-update) | async-done | bytes 11534352 | tf_op jit(solution)/shard_map/all_gather | solution.py:118
  342.3 97.2 %all-gather.17.cloned.1.call-done = bf16[2816,2048]{1,0:T(8,128)(2,1)} async-done(((bf16[2816,128]{1,0:T(8,128)(2,1)}), bf16[2816,2048]{1,0:T(8,128)(2,1)}) %all-gather.17.cloned.1.call-update) | async-done | bytes 11534352 | tf_op jit(solution)/shard_map/all_gather | solution.py:122
  439.4 13.9 %convolution_convert_fusion = bf16[192,2048]{1,0:T(8,128)(2,1)} fusion(bf16[2816,2048]{1,0:T(8,128)(2,1)} %all-gather.17.cloned.1.call-done, bf16[192,2048]{1,0:T(8,128)(2,1)S(1)} %all_gather.24, bf16[2048,2816]{1,0:T(8,128)(2,1)} %all-gather.15.cloned.1.call-done, f32[192,2816]{1,0:T(8,128)} %fusion.30), kind=kOutput, calls=%fused_computation.25 | convolution fusion | flops 4432822272 | bytes 26804224 | tf_op jit(solution)/shard_map/dot_general | solution.py:121
  453.3 15.8 %reduce-scatter.2.cloned.1.call-done = bf16[96,2048]{1,0:T(8,128)(2,1)} async-done(((bf16[192,2048]{1,0:T(8,128)(2,1)}), bf16[96,2048]{1,0:T(8,128)(2,1)}) %reduce-scatter.2.cloned.1.call-update) | async-done | bytes 393232 | tf_op jit(solution)/shard_map/reduce_scatter | solution.py:124
  469.2 1.8 add_convert_fusion
  (59 shorter events, 0.8 us)
Async XLA Ops:
  6.5 6.3 %copy-start.2 = (bf16[192,512]{1,0:T(8,128)(2,1)S(1)}, bf16[192,512]{1,0:T(8,128)(2,1)}, u32[]{:S(2)}) copy-start(bf16[192,512]{1,0:T(8,128)(2,1)} %param.13) | copy-start | bytes 589828
  6.5 45.4 %all-gather.7.cloned.1.call-start = ((), (), s32[]{:S(2)}) async-start(), calls=%async_computation.2 | async-start | bytes 1671168 | tf_op jit(solution)/shard_map/all_gather | solution.py:64
  8.4 4.6 copy-start.4
  9.5 83.1 %all-gather.9.cloned.1.call-start = ((), (), s32[]{:S(2)}) async-start(), calls=%async_computation.3 | async-start | bytes 1671168 | tf_op jit(solution)/shard_map/all_gather | solution.py:65
  10.2 141.5 %all-gather.11.cloned.1.call-start = ((), (), s32[]{:S(2)}) async-start(), calls=%async_computation.4 | async-start | bytes 6291456 | tf_op jit(solution)/shard_map/all_gather | solution.py:104
  11.0 236.9 %all-gather.13.cloned.1.call-start = ((), (), s32[]{:S(2)}) async-start(), calls=%async_computation.5 | async-start | bytes 12255232 | tf_op jit(solution)/shard_map/all_gather | solution.py:114
  11.6 330.7 %all-gather.15.cloned.1.call-start = ((), (), s32[]{:S(2)}) async-start(), calls=%async_computation.6 | async-start | bytes 12255232 | tf_op jit(solution)/shard_map/all_gather | solution.py:118
  12.1 427.3 %all-gather.17.cloned.1.call-start = ((), (), s32[]{:S(2)}) async-start(), calls=%async_computation.7 | async-start | bytes 12255232 | tf_op jit(solution)/shard_map/all_gather | solution.py:122
  12.7 456.4 %reduce-scatter.2.cloned.1.call-start = ((), (), s32[]{:S(2)}) async-start(), calls=%async_computation.8 | async-start | bytes 1179648 | tf_op jit(solution)/shard_map/reduce_scatter | solution.py:124
  102.3 1.1 copy-start
  105.2 0.8 copy-start.1
  107.7 1.0 copy-start
  110.5 0.8 copy-start.1
  113.0 1.0 copy-start
  115.9 0.8 copy-start.1
  118.4 1.0 copy-start
  121.2 0.8 copy-start.1
  123.8 1.0 copy-start
  126.6 0.8 copy-start.1
  129.1 1.0 copy-start
  132.0 0.8 copy-start.1
  134.2 20.7 %copy-start.3 = (f32[2048]{0:T(1024)S(1)}, f32[2048]{0:T(1024)}, u32[]{:S(2)}) copy-start(f32[2048]{0:T(1024)} %param.20) | copy-start | bytes 24580
Sparse Core Ops, SparseCore 0:
  9.6 42.3 all-gather.6
  54.3 38.2 all-gather.8
  94.1 57.5 all-gather.10
  153.9 93.9 all-gather.12
  250.0 92.2 all-gather.14
  344.3 95.1 all-gather.16
  453.4 15.6 reduce-scatter.1
where the time goes:
time: 479 us; the launch traced here: 478 us
  waiting for transfers between devices  362 us (76%)
  matrix products  46 us (10%)
  local copies, waits for them, and re-layouts  23.4 us (5%)
  blocking collectives  21.8 us (5%)
  between operations  13.7 us (3%)
  other arithmetic  10.2 us (2%)
    all_gather x1, waiting for transfers between devices, body(): lax.all_gather(w_down, 'sp', axis=1, tiled=True)  97.2 us
    all_gather x1, waiting for transfers between devices, body(): lax.all_gather(w_up, 'sp', axis=0, tiled=True)  86.4 us
    all_gather x1, waiting for transfers between devices, body(): lax.all_gather(w_gate, 'sp', axis=0, tiled=True)  81.3 us
    all_gather x1, waiting for transfers between devices, body(): key_piece = lax.all_gather(k_rot, 'sp', axis=0, tiled=True)  38.7 us
    all_gather x1, waiting for transfers between devices, body(): value_piece = lax.all_gather(values, 'sp', axis=0, tiled=True)  32.7 us
    reduce_scatter x1, waiting for transfers between devices, body(): lax.psum_scatter(terms.astype(jnp.bfloat16), 'tp', scatter_dimension=0, t...  15.8 us
    dot_general x1, matrix products, body(): jnp.dot(hidden, lax.all_gather(w_down, 'sp', axis=1, tiled=True), preferr...  13.9 us
    all_gather x1, blocking collectives, body(): gathered = lax.all_gather(normed, 'tp', axis=0, tiled=True)  11.5 us
  transfers between devices with their start and end apart: 7, of which 7 were waited for; matrix products, arithmetic and copies ran while one was open for 12% of the time, Pallas kernels for 0%

commit v1 on v0

--- a/solution.py
+++ b/solution.py
@@ -61,8 +61,11 @@
         jnp.zeros((kv_heads, q_group, tok_rows, head_size), jnp.float32),
     )
     running = start_state
-    key_piece = lax.all_gather(k_rot, "sp", axis=0, tiled=True)
-    value_piece = lax.all_gather(values, "sp", axis=0, tiled=True)
+    key_piece, value_piece = jnp.split(
+        lax.all_gather(jnp.concatenate([k_rot, values], axis=1), "sp", axis=0, tiled=True),
+        [k_rot.shape[1]],
+        axis=1,
+    )
     piece_len = key_piece.shape[0]
     block_len = math.gcd(piece_len, 512)
     blocks = piece_len // block_len

time: 479 us -> 443 us (0.925)
  waiting for transfers between devices: 362 us -> 325 us
  local copies, waits for them, and re-layouts: 23.4 us -> 28.2 us
    all_gather x2 -> x1, waiting for transfers between devices: 71.4 us -> 45.1 us  [body(): lax.all_gather(jnp.concatenate([k_rot, values], axis=1), 'sp', axis=0, ti...]
    all_gather x1, waiting for transfers between devices: 7.22 us -> 0.02 us  [body(): lax.all_gather(w_out, 'tp', axis=0, tiled=True)]
  transfers between devices with their start and end apart: 7 -> 6, of which waited for: 7 -> 5; matrix products, arithmetic and copies ran while one was open for 12% -> 13% of each run, Pallas kernels for 0% -> 0%
where the time goes in v1:
time: 443 us; the launch traced here: 442 us
  waiting for transfers between devices  325 us (73%)
  matrix products  45.9 us (10%)
  local copies, waits for them, and re-layouts  28.2 us (6%)
  blocking collectives  18.6 us (4%)
  between operations  13.7 us (3%)
  other arithmetic  10.3 us (2%)
    all_gather x1, waiting for transfers between devices, body(): lax.all_gather(w_down, 'sp', axis=1, tiled=True)  97.2 us
    all_gather x1, waiting for transfers between devices, body(): lax.all_gather(w_up, 'sp', axis=0, tiled=True)  86.4 us
    all_gather x1, waiting for transfers between devices, body(): lax.all_gather(w_gate, 'sp', axis=0, tiled=True)  78.1 us
    all_gather x1, waiting for transfers between devices, body(): lax.all_gather(jnp.concatenate([k_rot, values], axis=1), 'sp', axis=0, ti...  45.1 us
    reduce_scatter x1, waiting for transfers between devices, body(): lax.psum_scatter(terms.astype(jnp.bfloat16), 'tp', scatter_dimension=0, t...  15.8 us
    dot_general x1, matrix products, body(): jnp.dot(hidden, lax.all_gather(w_down, 'sp', axis=1, tiled=True), preferr...  13.9 us
    all_gather x1, blocking collectives, body(): gathered = lax.all_gather(normed, 'tp', axis=0, tiled=True)  11.1 us
    dot_general x6, matrix products, update(): jnp.einsum('hgqk,khd->hgqd', weights.astype(jnp.bfloat16), value_block, p...  10.8 us
  transfers between devices with their start and end apart: 6, of which 5 were waited for; matrix products, arithmetic and copies ran while one was open for 13% of the time, Pallas kernels for 0%

profile of v1, /device:TPU:0, one launch (start us, length us, event | category | flops | bytes accessed | tf_op | source)
XLA Modules:
  0.0 442.3 jit_solution(7349792426445212488)
XLA Ops:
  6.6 1.0 copy.23
  7.6 1.0 copy.24
  8.6 0.7 fusion.24
  9.4 0.2 multiply_cosine_fusion.1
  9.7 0.8 copy.25
  10.6 0.7 all-gather.8.cloned.1.call-update
  11.4 0.7 all-gather.10.cloned.1.call-update
  12.1 0.5 all-gather.12.cloned.1.call-update
  12.7 0.5 all-gather.14.cloned.1.call-update
  13.3 0.1 copy.27
  13.4 0.1 fusion.21
  13.5 0.1 fusion.22
  13.7 0.1 subtract_convert_fusion.1
  13.8 45.1 %all-gather.6.cloned.1.call-done = bf16[3072,512]{1,0:T(8,128)(2,1)} async-done(((bf16[192,512]{1,0:T(8,128)(2,1)}), bf16[3072,512]{1,0:T(8,128)(2,1)}) %all-gather.6.cloned.1.call-update) | async-done | bytes 3145744 | tf_op jit(solution)/shard_map/all_gather | solution.py:65
  58.9 3.7 fusion.30
  62.6 4.7 %reshape.207 = bf16[6,512,4,64]{3,2,1,0:T(4,128)(2,1)S(1)} reshape(bf16[3072,256]{1,0:T(8,128)(2,1)} %get-tuple-element.102) | data formatting | bytes 3145728 | tf_op jit(solution)/shard_map/reshape | solution.py:72
  67.3 3.3 copy.29
  70.6 4.6 %reshape.208 = bf16[6,512,4,64]{3,2,1,0:T(4,128)(2,1)S(1)} reshape(bf16[3072,256]{1,0:T(8,128)(2,1)} %get-tuple-element.101) | data formatting | bytes 3145728 | tf_op jit(solution)/shard_map/reshape | solution.py:73
  75.2 3.3 copy.30
  78.6 32.2 %while.15 = (s32[]{:T(128)}, f32[4,2,192]{2,1,0:T(2,128)S(1)}, f32[4,2,192]{2,1,0:T(2,128)S(1)}, f32[4,2,192,64]{2,3,1,0:T(8,128)}, bf16[6,512,4,64]{1,3,2,0:T(8...) while((s32[]{:T(128)}, f32[4,2,192]{2,1,0:T(2,128)S(1)}, ...), condition=%wide.region_5.6_spmd.clone, body=%wide.region_2.5_spmd.clone.sunk | while | flops 207920640 | bytes 14189729 | solution.py:96
  78.6 1.7 bitcast_reduce_fusion.2
  80.3 0.9 fusion.51
  81.2 0.1 copy-done
  81.3 1.8 fusion.53
  83.1 0.8 copy-done.1
  83.9 1.7 bitcast_reduce_fusion.2
  85.6 0.9 fusion.51
  86.6 0.1 copy-done
  86.7 1.8 fusion.53
  88.5 0.8 copy-done.1
  89.3 1.7 bitcast_reduce_fusion.2
  91.0 0.9 fusion.51
  92.0 0.1 copy-done
  92.0 1.8 fusion.53
  93.8 0.8 copy-done.1
  94.7 1.7 bitcast_reduce_fusion.2
  96.4 0.9 fusion.51
  97.3 0.1 copy-done
  97.4 1.8 fusion.53
  99.2 0.8 copy-done.1
  100.0 1.7 bitcast_reduce_fusion.2
  101.7 0.9 fusion.51
  102.7 0.1 copy-done
  102.8 1.8 fusion.53
  104.6 0.8 copy-done.1
  105.4 1.7 bitcast_reduce_fusion.2
  107.1 0.9 fusion.51
  108.1 0.1 copy-done
  108.1 1.8 fusion.53
  109.9 0.8 copy-done.1
  110.7 1.1 fusion.25
  111.8 0.2 convert_element_type.65
  112.0 0.2 copy.31
  112.2 7.5 %all_to_all.16 = bf16[2,96,512]{2,1,0:T(8,128)(2,1)S(1)} all-to-all(bf16[2,96,512]{2,1,0:T(8,128)(2,1)S(1)} %copy.31), channel_id=1, replica_groups=mesh['sp'=16,'tp'=2] {'tp'}, dimensions={0} | all-to-all | bytes 393216 | tf_op jit(solution)/shard_map/all_to_all | solution.py:104
  119.8 3.2 multiply_reduce_fusion
  123.0 0.1 multiply_convert_fusion
  123.1 11.1 %all_gather.20 = bf16[192,2048]{1,0:T(8,128)(2,1)S(1)} all-gather(bf16[96,2048]{1,0:T(8,128)(2,1)S(1)} %multiply_convert_fusion), channel_id=1, replica_groups=mesh['sp'=16,'tp'=2] {'tp'}, dimensions={0}, use_global_device_ids=true | all-gather | bytes 1179648 | tf_op jit(solution)/shard_map/all_gather | solution.py:113
  134.2 78.1 %all-gather.10.cloned.1.call-done = bf16[2048,2816]{1,0:T(8,128)(2,1)} async-done(((bf16[128,2816]{1,0:T(8,128)(2,1)}), bf16[2048,2816]{1,0:T(8,128)(2,1)}) %all-gather.10.cloned.1.call-update) | async-done | bytes 11534352 | tf_op jit(solution)/shard_map/all_gather | solution.py:117
  212.3 8.0 %fusion.31 = f32[192,2816]{1,0:T(8,128)} fusion(bf16[192,2048]{1,0:T(8,128)(2,1)S(1)} %all_gather.20, bf16[2048,2816]{1,0:T(8,128)(2,1)} %all-gather.10.cloned.1.call-done), kind=kOutput, calls=%fused_computation.71 | convolution fusion | flops 2214592512 | bytes 14483456 | tf_op jit(solution)/shard_map/dot_general | solution.py:115
  220.3 86.4 %all-gather.12.cloned.1.call-done = bf16[2048,2816]{1,0:T(8,128)(2,1)} async-done(((bf16[128,2816]{1,0:T(8,128)(2,1)}), bf16[2048,2816]{1,0:T(8,128)(2,1)}) %all-gather.12.cloned.1.call-update) | async-done | bytes 11534352 | tf_op jit(solution)/shard_map/all_gather | solution.py:121
  306.7 97.2 %all-gather.14.cloned.1.call-done = bf16[2816,2048]{1,0:T(8,128)(2,1)} async-done(((bf16[2816,128]{1,0:T(8,128)(2,1)}), bf16[2816,2048]{1,0:T(8,128)(2,1)}) %all-gather.14.cloned.1.call-update) | async-done | bytes 11534352 | tf_op jit(solution)/shard_map/all_gather | solution.py:125
  403.9 13.9 %convolution_convert_fusion = bf16[192,2048]{1,0:T(8,128)(2,1)} fusion(bf16[2816,2048]{1,0:T(8,128)(2,1)} %all-gather.14.cloned.1.call-done, bf16[192,2048]{1,0:T(8,128)(2,1)S(1)} %all_gather.20, bf16[2048,2816]{1,0:T(8,128)(2,1)} %all-gather.12.cloned.1.call-done, f32[192,2816]{1,0:T(8,128)} %fusion.31), kind=kOutput, calls=%fused_computation.25 | convolution fusion | flops 4432822272 | bytes 26804224 | tf_op jit(solution)/shard_map/dot_general | solution.py:124
  417.8 15.8 %reduce-scatter.2.cloned.1.call-done = bf16[96,2048]{1,0:T(8,128)(2,1)} async-done(((bf16[192,2048]{1,0:T(8,128)(2,1)}), bf16[96,2048]{1,0:T(8,128)(2,1)}) %reduce-scatter.2.cloned.1.call-update) | async-done | bytes 393232 | tf_op jit(solution)/shard_map/reduce_scatter | solution.py:127
  433.6 1.8 add_convert_fusion
  (59 shorter events, 0.8 us)
Async XLA Ops:
  6.5 52.3 %all-gather.6.cloned.1.call-start = ((), (), s32[]{:S(2)}) async-start(), calls=%async_computation.2 | async-start | bytes 3342336 | tf_op jit(solution)/shard_map/all_gather | solution.py:65
  9.4 3.9 copy-start.2
  9.7 3.9 copy-start.4
  10.6 109.2 %all-gather.8.cloned.1.call-start = ((), (), s32[]{:S(2)}) async-start(), calls=%async_computation.3 | async-start | bytes 6291456 | tf_op jit(solution)/shard_map/all_gather | solution.py:107
  11.3 201.0 %all-gather.10.cloned.1.call-start = ((), (), s32[]{:S(2)}) async-start(), calls=%async_computation.4 | async-start | bytes 12255232 | tf_op jit(solution)/shard_map/all_gather | solution.py:117
  12.0 294.7 %all-gather.12.cloned.1.call-start = ((), (), s32[]{:S(2)}) async-start(), calls=%async_computation.5 | async-start | bytes 12255232 | tf_op jit(solution)/shard_map/all_gather | solution.py:121
  12.6 391.3 %all-gather.14.cloned.1.call-start = ((), (), s32[]{:S(2)}) async-start(), calls=%async_computation.6 | async-start | bytes 12255232 | tf_op jit(solution)/shard_map/all_gather | solution.py:125
  13.2 420.4 %reduce-scatter.2.cloned.1.call-start = ((), (), s32[]{:S(2)}) async-start(), calls=%async_computation.7 | async-start | bytes 1179648 | tf_op jit(solution)/shard_map/reduce_scatter | solution.py:127
  80.3 1.0 copy-start
  83.1 0.8 copy-start.1
  85.6 1.0 copy-start
  88.5 0.8 copy-start.1
  91.0 1.0 copy-start
  93.8 0.8 copy-start.1
  96.3 1.0 copy-start
  99.2 0.8 copy-start.1
  101.7 1.0 copy-start
  104.6 0.8 copy-start.1
  107.1 1.0 copy-start
  109.9 0.8 copy-start.1
  112.2 10.8 %copy-start.3 = (f32[2048]{0:T(1024)S(1)}, f32[2048]{0:T(1024)}, u32[]{:S(2)}) copy-start(f32[2048]{0:T(1024)} %param.20) | copy-start | bytes 24580
Sparse Core Ops, SparseCore 0:
  10.7 48.1 all-gather.5
  60.4 55.0 all-gather.7
  117.8 94.4 all-gather.9
  214.5 92.2 all-gather.11
  308.7 95.1 all-gather.13
  417.9 15.6 reduce-scatter.1
